TPU v7x, 32 devices: a whole 2x2x4 slice. The times are simulated.
32 devices in a mesh: ep: 8 (over z, x), tp: 4 (over y, core).
Axes of the slice: x: 2, y: 2, z: 4, core: 2. Of those that a mesh axis runs over, the one named last changes fastest.
Arguments:
- tokens: bfloat16 [192, 2048], P('ep'), may hold values from -12 to 12
- state: float32 [192, 16, 128, 256], P('ep', 'tp'), may hold values from -6 to 6
- w_query: bfloat16 [2048, 2048], P(None, 'tp'), may hold values from -0.125 to 0.125
- w_key: bfloat16 [2048, 2048], P(None, 'tp'), may hold values from -0.125 to 0.125
- w_value: bfloat16 [2048, 4096], P(None, 'tp'), may hold values from -0.125 to 0.125
- w_outgate: bfloat16 [2048, 4096], P(None, 'tp'), may hold values from -0.125 to 0.125
- decay_down: bfloat16 [2048, 16], replicated, may hold values from -0.125 to 0.125
- decay_up: bfloat16 [16, 2048], P(None, 'tp'), may hold values from -9 to 9
- decay_bias: float32 [2048], P('tp'), may hold values from -6 to 4
- head_gain: float32 [256], replicated, may hold values from 0.1 to 1.9
- w_output: bfloat16 [4096, 2048], P('tp'), may hold values from -0.09375 to 0.09375
- norm1_gain: float32 [2048], P('tp'), may hold values from 0.1 to 1.9
- route_ids: int32 [192, 6], P('ep'), may hold values from 0 to 31, all different within a row; in each aligned block of 24 rows (0 to 23, 24 to 47, ...) at most 5 rows name the same one
- route_weight: float32 [192, 6], P('ep'), may hold values from 0.1 to 1
- exp_gate: bfloat16 [32, 2048, 512], P('ep', 'tp'), may hold values from -0.125 to 0.125
- exp_up: bfloat16 [32, 2048, 512], P('ep', 'tp'), may hold values from -0.125 to 0.125
- exp_down: bfloat16 [32, 512, 2048], P('ep', None, 'tp'), may hold values from -0.25 to 0.25
- sh_gate: bfloat16 [2048, 512], P('tp'), may hold values from -0.125 to 0.125
- sh_up: bfloat16 [2048, 512], P('tp'), may hold values from -0.125 to 0.125
- sh_down: bfloat16 [512, 2048], P(None, 'tp'), may hold values from -0.25 to 0.25
- norm2_gain: float32 [2048], P('tp'), may hold values from 0.1 to 1.9
Outputs:
- layer_out: bfloat16 [192, 2048], P('ep', 'tp')
Inputs may be any that keep to these rules, and one draw needn't show every extreme that they name: `route_ids`: each row names 6 different experts. Among the rows of one index of ep (aligned blocks of 24 rows) no expert is named by more than 5 rows, and in some blocks one expert is named by exactly 5.
All inputs are finite; a program needn't handle non-finite values.
Results may differ from a plain program's by a relative error of at most 0.02.
Values may be sent and summed in bfloat16 or wider, within the bound.
A program may use at most 64 MiB of HBM per device.

v0:
```python
import jax
import jax.numpy as jnp
from jax import lax
from jax.sharding import PartitionSpec as P

res_scale = 2.0**0.5
decay_tau = 16.0
norm_eps = 1e-05


def settle(values):
    return lax.optimization_barrier(values.astype(jnp.bfloat16)).astype(jnp.float32)


def project(left, right):
    return jnp.dot(left, right, preferred_element_type=jnp.float32)


def apply_norm(values, sums, squares, width, gain):
    mean_val = sums[:, None] / width
    spread = squares[:, None] / width - mean_val * mean_val
    return (values - mean_val) * lax.rsqrt(spread + norm_eps) * gain


def per_device(
    tokens,
    state,
    w_query,
    w_key,
    w_value,
    w_outgate,
    decay_down,
    decay_up,
    decay_bias,
    head_gain,
    w_output,
    norm1_gain,
    route_ids,
    route_weight,
    exp_gate,
    exp_up,
    exp_down,
    sh_gate,
    sh_up,
    sh_down,
    norm2_gain,
):
    row_count, width = tokens.shape
    head_count, key_dim, val_dim = (state.shape[1], state.shape[2], state.shape[3])
    tp_count = lax.axis_size("tp")
    ep_count = lax.axis_size("ep")
    col_count = width // tp_count
    col_start = lax.axis_index("tp") * col_count
    queries = settle(project(tokens, w_query)).reshape(
        row_count, head_count, key_dim
    ) * key_dim ** (-0.5)
    key_rows = settle(project(tokens, w_key)).reshape(row_count, head_count, key_dim)
    values = settle(project(tokens, w_value)).reshape(row_count, head_count, val_dim)
    gate_pre = settle(project(tokens, w_outgate)).reshape(row_count, head_count, val_dim)
    decay_low = lax.optimization_barrier(project(tokens, decay_down).astype(jnp.bfloat16))
    log_decay = (jax.nn.log_sigmoid(project(decay_low, decay_up) + decay_bias) / decay_tau).reshape(
        row_count, head_count, key_dim
    )
    carried = jnp.einsum(
        "bhk,bhkv->bhv", queries * jnp.exp(log_decay), state, precision=lax.Precision.HIGHEST
    )
    attended = carried + jnp.sum(queries * key_rows, -1, keepdims=True) * values
    inv_norm = lax.rsqrt(jnp.mean(attended * attended, -1, keepdims=True) + norm_eps)
    head_out = (
        (attended * inv_norm * head_gain * jax.nn.silu(gate_pre))
        .astype(jnp.bfloat16)
        .reshape(row_count, head_count * val_dim)
    )
    partial_out = project(head_out, w_output)
    mixed = settle(
        lax.psum_scatter(
            partial_out.astype(jnp.bfloat16), "tp", scatter_dimension=1, tiled=True
        ).astype(jnp.float32)
    )
    own_tokens = lax.dynamic_slice_in_dim(tokens, col_start, col_count, 1).astype(jnp.float32)
    own_resid = res_scale * own_tokens + mixed
    first_sums, first_squares = lax.psum(
        (jnp.sum(own_resid, -1), jnp.sum(own_resid * own_resid, -1)), "tp"
    )
    normed_mid = apply_norm(own_resid, first_sums, first_squares, width, norm1_gain)
    normed_mid = lax.optimization_barrier(normed_mid.astype(jnp.bfloat16))
    top_count = route_ids.shape[1]
    local_count = exp_gate.shape[0]
    expert_count = local_count * ep_count
    capacity = max(2, row_count * top_count // expert_count + 1)
    flat_ids = route_ids.reshape(row_count * top_count)
    onehot = (flat_ids[:, None] == jnp.arange(expert_count, dtype=jnp.int32)[None, :]).astype(
        jnp.int32
    )
    ranks = jnp.sum((jnp.cumsum(onehot, 0) - 1) * onehot, 1)
    slots = flat_ids * capacity + ranks
    placement = (
        slots[:, None] == jnp.arange(expert_count * capacity, dtype=jnp.int32)[None, :]
    ).astype(jnp.bfloat16)
    pair_rows = jnp.repeat(normed_mid, top_count, axis=0)
    outgoing = jnp.einsum(
        "ps,pc->sc", placement, pair_rows, preferred_element_type=jnp.float32
    ).astype(jnp.bfloat16)
    outgoing = outgoing.reshape(ep_count, local_count, capacity, col_count)
    incoming = lax.all_to_all(outgoing, "ep", split_axis=0, concat_axis=0, tiled=True)
    gate_part = jnp.einsum("secd,edf->secf", incoming, exp_gate, preferred_element_type=jnp.float32)
    up_part = jnp.einsum("secd,edf->secf", incoming, exp_up, preferred_element_type=jnp.float32)
    shared_gate_part = project(normed_mid, sh_gate)
    shared_up_part = project(normed_mid, sh_up)
    gate_sum, up_sum, shared_gate_sum, shared_up_sum = (
        lax.psum(gate_part.astype(jnp.bfloat16), "tp").astype(jnp.float32),
        lax.psum(up_part.astype(jnp.bfloat16), "tp").astype(jnp.float32),
        lax.psum(shared_gate_part.astype(jnp.bfloat16), "tp").astype(jnp.float32),
        lax.psum(shared_up_part.astype(jnp.bfloat16), "tp").astype(jnp.float32),
    )
    inner = (jax.nn.silu(settle(gate_sum)) * settle(up_sum)).astype(jnp.bfloat16)
    shared_inner = (jax.nn.silu(settle(shared_gate_sum)) * settle(shared_up_sum)).astype(
        jnp.bfloat16
    )
    expert_out = jnp.einsum(
        "secf,efd->secd", inner, exp_down, preferred_element_type=jnp.float32
    ).astype(jnp.bfloat16)
    returned = lax.all_to_all(expert_out, "ep", split_axis=0, concat_axis=0, tiled=True)
    picked = jnp.einsum(
        "ps,sc->pc",
        placement,
        returned.reshape(expert_count * capacity, col_count),
        preferred_element_type=jnp.float32,
    )
    routed = jnp.sum(picked.reshape(row_count, top_count, col_count) * route_weight[:, :, None], 1)
    mixture = routed + project(shared_inner, sh_down)
    out_resid = res_scale * normed_mid.astype(jnp.float32) + mixture
    last_sums, last_squares = lax.psum(
        (jnp.sum(out_resid, -1), jnp.sum(out_resid * out_resid, -1)), "tp"
    )
    return apply_norm(out_resid, last_sums, last_squares, width, norm2_gain).astype(jnp.bfloat16)


def solution(mesh):
    in_specs = (
        P("ep", None),
        P("ep", "tp", None, None),
        P(None, "tp"),
        P(None, "tp"),
        P(None, "tp"),
        P(None, "tp"),
        P(),
        P(None, "tp"),
        P("tp"),
        P(),
        P("tp", None),
        P("tp"),
        P("ep", None),
        P("ep", None),
        P("ep", "tp", None),
        P("ep", "tp", None),
        P("ep", None, "tp"),
        P("tp", None),
        P("tp", None),
        P(None, "tp"),
        P("tp"),
    )
    out_specs = P("ep", "tp")
    return jax.shard_map(
        per_device, mesh=mesh, in_specs=in_specs, out_specs=out_specs, check_vma=False
    )
```

profile of v0, /device:TPU:0, one launch (start us, length us, event | category | flops | bytes accessed | tf_op | source)
XLA Modules:
  0.0 142.7 jit_solution(752916315707150363)
XLA Ops:
  6.6 2.2 %convolution_convert_fusion.5 = bf16[24,512]{1,0:T(8,128)(2,1)S(1)} fusion(bf16[24,2048]{1,0:T(8,128)(2,1)} %param.21, bf16[2048,512]{1,0:T(8,128)(2,1)} %param.23), kind=kOutput, calls=%fused_computation.23 | convolution fusion | flops 50343936 | bytes 2220032 | tf_op jit(solution)/shard_map/dot_general | solution.py:16
  8.9 0.2 fusion.49
  9.2 2.0 %convolution_convert_fusion.4 = bf16[24,512]{1,0:T(8,128)(2,1)S(1)} fusion(bf16[24,2048]{1,0:T(8,128)(2,1)S(1)} %copy-done.1, bf16[2048,512]{1,0:T(8,128)(2,1)} %param.24), kind=kOutput, calls=%fused_computation.22 | convolution fusion | flops 50343936 | bytes 2220032 | tf_op jit(solution)/shard_map/dot_general | solution.py:16
  11.2 2.8 %convolution_convert_fusion.3 = bf16[24,1024]{1,0:T(8,128)(2,1)S(1)} fusion(bf16[24,2048]{1,0:T(8,128)(2,1)S(1)} %copy-done.1, bf16[2048,1024]{1,0:T(8,128)(2,1)} %param.25), kind=kOutput, calls=%fused_computation.17 | convolution fusion | flops 100687872 | bytes 4341760 | tf_op jit(solution)/shard_map/dot_general | solution.py:16
  14.1 8.6 %fusion.59 = f32[24,4,1,256]{3,2,1,0:T(1,128)S(1)} fusion(f32[24,4,128,1]{2,3,1,0:T(1,128)S(1)} %bitcast.80, f32[24,4,128,256]{3,2,1,0:T(8,128)} %param.22), kind=kOutput, calls=%fused_computation.88 | convolution fusion | flops 37748736 | bytes 12730368 | tf_op jit(solution)/shard_map/bhk,bhkv->bhv/dot_general | solution.py:64
  22.8 0.2 multiply_reduce_fusion
  23.0 2.8 %convolution_convert_fusion.2 = bf16[24,1024]{1,0:T(8,128)(2,1)S(1)} fusion(bf16[24,2048]{1,0:T(8,128)(2,1)S(1)} %copy-done.1, bf16[2048,1024]{1,0:T(8,128)(2,1)} %param.26), kind=kOutput, calls=%fused_computation.16 | convolution fusion | flops 100687872 | bytes 4341760 | tf_op jit(solution)/shard_map/dot_general | solution.py:16
  26.1 3.5 %convolution_convert_fusion = bf16[24,2048]{1,0:T(8,128)(2,1)} fusion(bf16[24,1024]{1,0:T(8,128)(2,1)S(1)} %bitcast.81, bf16[1024,2048]{1,0:T(8,128)(2,1)} %param.31), kind=kOutput, calls=%fused_computation | convolution fusion | flops 100712448 | bytes 4341760 | tf_op jit(solution)/shard_map/dot_general | solution.py:16
  29.9 0.6 reduce-window.6
  30.4 0.2 slice_reduce_fusion
  30.8 21.4 %reduce-scatter.2.cloned.1.call-done = bf16[24,512]{1,0:T(8,128)(2,1)} async-done(((bf16[24,2048]{1,0:T(8,128)(2,1)}), bf16[24,512]{1,0:T(8,128)(2,1)}) %reduce-scatter.2.cloned.1.call-update) | async-done | bytes 24592 | tf_op jit(solution)/shard_map/reduce_scatter | solution.py:76
  52.2 0.9 fusion.51
  53.0 5.8 %all-reduce.2 = (f32[24]{0:T(128)S(1)}, f32[24]{0:T(128)S(1)}) all-reduce(f32[24]{0:T(128)S(1)} %get-tuple-element.6, f32[24]{0:T(128)S(1)} %get-tuple-element.5), channel_id=1, replica_groups=mesh['ep'=8,'tp'=4] {'tp'}, use_global_device_ids=true, to_apply=%region_6.7 | all-reduce | flops 48 | bytes 384 | tf_op jit(solution)/shard_map/psum | solution.py:82
  58.8 0.8 multiply_convert_fusion.1
  59.7 0.3 convolution_convert_fusion.1
  60.1 0.7 copy.52
  60.9 5.7 %all-to-all-start = ((bf16[8,4,5,512]{3,1,2,0:T(4,128)(2,1)}), bf16[8,4,5,512]{3,1,2,0:T(4,128)(2,1)S(1)}, u32[]{:S(2)}, u32[]{:S(2)}) async-start(bf16[8,4,5,512]{3,1,2,0:T(4,128)(2,1)} %copy.52), calls=%async_computation.1 | async-start | bytes 327680 | tf_op jit(solution)/shard_map/all_to_all | solution.py:105
  66.7 7.3 %all-to-all-done = bf16[8,4,5,512]{3,1,2,0:T(4,128)(2,1)S(1)} async-done(((bf16[8,4,5,512]{3,1,2,0:T(4,128)(2,1)}), bf16[8,4,5,512]{3,1,2,0:T(4,128)(2,1)S(1)}, u32[]{:S(2)}, u32[]{:S(2)}) %all-to-all-start) | async-done | bytes 163872 | tf_op jit(solution)/shard_map/all_to_all | solution.py:105
  74.1 1.1 fusion.19
  75.2 0.6 copy-done.2
  75.8 1.1 fusion.22
  76.9 29.9 %all-reduce.7.cloned.1.call-done = (bf16[8,4,5,512]{3,0,2,1:T(8,128)(2,1)}, bf16[8,4,5,512]{3,0,2,1:T(8,128)(2,1)}) async-done(((bf16[8,4,5,512]{3,0,2,1:T(8,128)(2,1)}, bf16[8,4,5,512]{3,0,2,1:T(8,128)(2,1)}), (bf16[8,4,5,512]{3,0,2,1:T(8,128)(2,1)}, bf16[8,4,5,512]{3,0,2,1:T(8,128)(2,1)})) %all-reduce.7.cloned.1.call-update) | async-done | bytes 327696 | tf_op jit(solution)/shard_map/psum | solution.py:112
  106.8 2.2 %fusion.16 = bf16[8,4,5,512]{3,0,2,1:T(8,128)(2,1)S(1)} fusion(bf16[4,512,512]{2,1,0:T(8,128)(2,1)} %param.37, bf16[8,4,5,512]{3,0,2,1:T(8,128)(2,1)} %get-tuple-element.15, bf16[8,4,5,512]{3,0,2,1:T(8,128)(2,1)} %get-tuple-element.16), kind=kOutput, calls=%fused_computation.13 | convolution fusion | flops 84623360 | bytes 2588672 | tf_op jit(solution)/shard_map/secf,efd->secd/dot_general | solution.py:120
  109.0 0.7 copy.55
  109.7 5.5 %all-to-all-start.1 = ((bf16[8,4,5,512]{3,1,2,0:T(4,128)(2,1)}), bf16[8,4,5,512]{3,1,2,0:T(4,128)(2,1)S(1)}, u32[]{:S(2)}, u32[]{:S(2)}) async-start(bf16[8,4,5,512]{3,1,2,0:T(4,128)(2,1)} %copy.55), calls=%async_computation.2 | async-start | bytes 327680 | tf_op jit(solution)/shard_map/all_to_all | solution.py:123
  115.2 0.2 convolution_convert_fusion.6
  115.4 1.2 convolution_convert_fusion.7
  116.7 10.9 %all-reduce.3 = (bf16[24,512]{1,0:T(8,128)(2,1)S(1)}, bf16[24,512]{1,0:T(8,128)(2,1)S(1)}) all-reduce(bf16[24,512]{1,0:T(8,128)(2,1)S(1)} %convolution_convert_fusion.6, bf16[24,512]{1,0:T(8,128)(2,1)S(1)} %convolution_convert_fusion.7), channel_id=1, replica_groups=mesh['ep'=8,'tp'=4] {'tp'}, use_global_device_ids=true, to_apply=%region_14.15 | all-reduce | flops 24576 | bytes 98304 | tf_op jit(solution)/shard_map/psum | solution.py:114
  127.7 0.2 fusion.15
  127.9 1.3 fusion.58
  129.3 5.9 %all-reduce.1 = (f32[24]{0:T(128)S(1)}, f32[24]{0:T(128)S(1)}) all-reduce(f32[24]{0:T(128)S(1)} %get-tuple-element.8, f32[24]{0:T(128)S(1)} %get-tuple-element.7), channel_id=1, replica_groups=mesh['ep'=8,'tp'=4] {'tp'}, use_global_device_ids=true, to_apply=%region_18.19 | all-reduce | flops 48 | bytes 384 | tf_op jit(solution)/shard_map/psum | solution.py:133
  135.2 0.7 multiply_convert_fusion
  (57 shorter events, 1.6 us)
Async XLA Ops:
  6.5 67.6 %copy-start = (bf16[4,512,512]{2,1,0:T(8,128)(2,1)S(1)}, bf16[4,512,512]{2,1,0:T(8,128)(2,1)}, u32[]{:S(2)}) copy-start(bf16[4,512,512]{2,1,0:T(8,128)(2,1)} %param.36) | copy-start | bytes 6291460
  6.5 2.2 %copy-start.1 = (bf16[24,2048]{1,0:T(8,128)(2,1)S(1)}, bf16[24,2048]{1,0:T(8,128)(2,1)}, u32[]{:S(2)}) copy-start(bf16[24,2048]{1,0:T(8,128)(2,1)} %param.21) | copy-start | bytes 294916
  6.5 2.2 %copy-start.4 = (bf16[2048,16]{0,1:T(8,128)(2,1)S(1)}, bf16[2048,16]{0,1:T(8,128)(2,1)}, u32[]{:S(2)}) copy-start(bf16[2048,16]{0,1:T(8,128)(2,1)} %param.27) | copy-start | bytes 196612
  6.5 2.4 %copy-start.9 = (bf16[16,512]{1,0:T(8,128)(2,1)S(1)}, bf16[16,512]{1,0:T(8,128)(2,1)}, u32[]{:S(2)}) copy-start(bf16[16,512]{1,0:T(8,128)(2,1)} %param.28) | copy-start | bytes 49156
  6.5 2.4 %copy-start.11 = (f32[512]{0:T(512)S(1)}, f32[512]{0:T(512)}, u32[]{:S(2)}) copy-start(f32[512]{0:T(512)} %param.29) | copy-start | bytes 6148
  6.5 45.6 %reduce-scatter.2.cloned.1.call-start = ((), (), s32[]{:S(2)}) async-start(), calls=%async_computation.3 | async-start | bytes 122880 | tf_op jit(solution)/shard_map/reduce_scatter | solution.py:76
  23.0 2.9 %copy-start.8 = (f32[256]{0:T(256)S(1)}, f32[256]{0:T(256)}, u32[]{:S(2)}) copy-start(f32[256]{0:T(256)} %param.30) | copy-start | bytes 3076
  26.1 3.5 %copy-start.5 = (s32[24,6]{0,1:T(8,128)S(1)}, s32[24,6]{0,1:T(8,128)}, u32[]{:S(2)}) copy-start(s32[24,6]{0,1:T(8,128)} %param.33) | copy-start | bytes 1732
  26.1 32.7 %copy-start.6 = (f32[512]{0:T(512)S(1)}, f32[512]{0:T(512)}, u32[]{:S(2)}) copy-start(f32[512]{0:T(512)} %param.32) | copy-start | bytes 6148
  60.9 13.2 %all-to-all-start = ((bf16[8,4,5,512]{3,1,2,0:T(4,128)(2,1)}), bf16[8,4,5,512]{3,1,2,0:T(4,128)(2,1)S(1)}, u32[]{:S(2)}, u32[]{:S(2)}) async-start(bf16[8,4,5,512]{3,1,2,0:T(4,128)(2,1)} %copy.52), calls=%async_computation.1 | async-start | bytes 327680 | tf_op jit(solution)/shard_map/all_to_all | solution.py:105
  66.5 40.2 %all-reduce.7.cloned.1.call-start = ((), (), s32[]{:S(2)}) async-start(), calls=%async_computation.4 | async-start | bytes 655360 | tf_op jit(solution)/shard_map/psum | solution.py:112
  74.1 1.7 %copy-start.2 = (bf16[4,512,512]{2,1,0:T(8,128)(2,1)S(1)}, bf16[4,512,512]{2,1,0:T(8,128)(2,1)}, u32[]{:S(2)}) copy-start(bf16[4,512,512]{2,1,0:T(8,128)(2,1)} %param.35) | copy-start | bytes 6291460
  76.8 38.4 %copy-start.3 = (bf16[512,512]{1,0:T(8,128)(2,1)S(1)}, bf16[512,512]{1,0:T(8,128)(2,1)}, u32[]{:S(2)}) copy-start(bf16[512,512]{1,0:T(8,128)(2,1)} %param.39) | copy-start | bytes 1572868
  106.8 20.9 %copy-start.10 = (f32[24,6]{0,1:T(8,128)S(1)}, f32[24,6]{0,1:T(8,128)}, u32[]{:S(2)}) copy-start(f32[24,6]{0,1:T(8,128)} %param.34) | copy-start | bytes 1732
  109.0 26.2 %copy-start.7 = (f32[512]{0:T(512)S(1)}, f32[512]{0:T(512)}, u32[]{:S(2)}) copy-start(f32[512]{0:T(512)} %param.41) | copy-start | bytes 6148
  109.7 17.8 %all-to-all-start.1 = ((bf16[8,4,5,512]{3,1,2,0:T(4,128)(2,1)}), bf16[8,4,5,512]{3,1,2,0:T(4,128)(2,1)S(1)}, u32[]{:S(2)}, u32[]{:S(2)}) async-start(bf16[8,4,5,512]{3,1,2,0:T(4,128)(2,1)} %copy.55), calls=%async_computation.2 | async-start | bytes 327680 | tf_op jit(solution)/shard_map/all_to_all | solution.py:123
Sparse Core Ops, SparseCore 0:
  29.7 22.3 reduce-scatter.1
  77.0 29.7 all-reduce.6
where the time goes:
time: 143 us
  waiting for transfers between devices  58.6 us (41%)
  matrix products  29.9 us (21%)
  blocking collectives  22.5 us (16%)
  between operations  13.7 us (10%)
  starting transfers between devices  11.3 us (8%)
  other arithmetic  3.59 us (3%)
  local copies, waits for them, and re-layouts  3.1 us (2%)
    psum x1, waiting for transfers between devices, per_device(): lax.psum(up_part.astype(jnp.bfloat16), 'tp').astype(jnp.float32)  29.9 us
    reduce_scatter x1, waiting for transfers between devices, per_device(): lax.psum_scatter(partial_out.astype(jnp.bfloat16), 'tp', scatter_dimensio...  21.4 us
    dot_general x10, matrix products, project(): return jnp.dot(left, right, preferred_element_type=jnp.float32)  16.4 us
    psum x1, blocking collectives, per_device(): lax.psum(shared_up_part.astype(jnp.bfloat16), 'tp').astype(jnp.float32)  10.9 us
    dot_general x1, matrix products, per_device(): jnp.einsum('bhk,bhkv->bhv', queries * jnp.exp(log_decay), state, precisio...  8.56 us
    all_to_all x1, waiting for transfers between devices, per_device(): lax.all_to_all(outgoing, 'ep', split_axis=0, concat_axis=0, tiled=True)  7.35 us
    psum x1, blocking collectives, per_device(): lax.psum((jnp.sum(out_resid, -1), jnp.sum(out_resid * out_resid, -1)), 'tp')  5.88 us
    psum x1, blocking collectives, per_device(): lax.psum((jnp.sum(own_resid, -1), jnp.sum(own_resid * own_resid, -1)), 'tp')  5.76 us
  transfers between devices with their start and end apart: 4, of which 3 were waited for; matrix products, arithmetic and copies ran while one was open for 2% of the time, Pallas kernels for 0%

commit v1 on v0

--- a/solution.py
+++ b/solution.py
@@ -109,7 +109,7 @@
     shared_up_part = project(normed_mid, sh_up)
     gate_sum, up_sum, shared_gate_sum, shared_up_sum = (
         lax.psum(gate_part.astype(jnp.bfloat16), "tp").astype(jnp.float32),
-        lax.psum(up_part.astype(jnp.bfloat16), "tp").astype(jnp.float32),
+        jnp.sum(lax.all_gather(up_part.astype(jnp.bfloat16), "tp"), axis=0).astype(jnp.float32),
         lax.psum(shared_gate_part.astype(jnp.bfloat16), "tp").astype(jnp.float32),
         lax.psum(shared_up_part.astype(jnp.bfloat16), "tp").astype(jnp.float32),
     )

time: 143 us -> 150 us (1.049)
  blocking collectives: 22.5 us -> 29.7 us
    all_gather x0 -> x1, blocking collectives: none -> 7.2 us  [per_device(): lax.all_gather(up_part.astype(jnp.bfloat16), 'tp')]
  transfers between devices with their start and end apart: 4 -> 4, of which waited for: 3 -> 3; matrix products, arithmetic and copies ran while one was open for 2% -> 3% of each run, Pallas kernels for 0% -> 0%
where the time goes in v1:
time: 150 us
  waiting for transfers between devices  58.6 us (39%)
  matrix products  30.2 us (20%)
  blocking collectives  29.7 us (20%)
  between operations  13.7 us (9%)
  starting transfers between devices  11.3 us (8%)
  other arithmetic  3.68 us (2%)
  local copies, waits for them, and re-layouts  2.52 us (2%)
    psum x1, waiting for transfers between devices, per_device(): lax.psum(gate_part.astype(jnp.bfloat16), 'tp').astype(jnp.float32)  29.9 us
    reduce_scatter x1, waiting for transfers between devices, per_device(): lax.psum_scatter(partial_out.astype(jnp.bfloat16), 'tp', scatter_dimensio...  21.4 us
    dot_general x10, matrix products, project(): return jnp.dot(left, right, preferred_element_type=jnp.float32)  17.5 us
    psum x1, blocking collectives, per_device(): lax.psum(shared_up_part.astype(jnp.bfloat16), 'tp').astype(jnp.float32)  10.9 us
    dot_general x1, matrix products, per_device(): jnp.einsum('bhk,bhkv->bhv', queries * jnp.exp(log_decay), state, precisio...  8.56 us
    all_to_all x1, waiting for transfers between devices, per_device(): lax.all_to_all(outgoing, 'ep', split_axis=0, concat_axis=0, tiled=True)  7.34 us
    all_gather x1, blocking collectives, per_device(): lax.all_gather(up_part.astype(jnp.bfloat16), 'tp')  7.2 us
    psum x1, blocking collectives, per_device(): lax.psum((jnp.sum(out_resid, -1), jnp.sum(out_resid * out_resid, -1)), 'tp')  5.87 us
  transfers between devices with their start and end apart: 4, of which 3 were waited for; matrix products, arithmetic and copies ran while one was open for 3% of the time, Pallas kernels for 0%

profile of v1, /device:TPU:0, one launch (start us, length us, event | category | flops | bytes accessed | tf_op | source)
XLA Modules:
  0.0 149.6 jit_solution(17431064973758879756)
XLA Ops:
  6.6 2.2 %convolution_convert_fusion.5 = bf16[24,512]{1,0:T(8,128)(2,1)S(1)} fusion(bf16[24,2048]{1,0:T(8,128)(2,1)} %param.21, bf16[2048,512]{1,0:T(8,128)(2,1)} %param.23), kind=kOutput, calls=%fused_computation.23 | convolution fusion | flops 50343936 | bytes 2220032 | tf_op jit(solution)/shard_map/dot_general | solution.py:16
  8.9 0.2 fusion.49
  9.2 2.0 %convolution_convert_fusion.4 = bf16[24,512]{1,0:T(8,128)(2,1)S(1)} fusion(bf16[24,2048]{1,0:T(8,128)(2,1)S(1)} %copy-done.1, bf16[2048,512]{1,0:T(8,128)(2,1)} %param.24), kind=kOutput, calls=%fused_computation.22 | convolution fusion | flops 50343936 | bytes 2220032 | tf_op jit(solution)/shard_map/dot_general | solution.py:16
  11.2 2.8 %convolution_convert_fusion.3 = bf16[24,1024]{1,0:T(8,128)(2,1)S(1)} fusion(bf16[24,2048]{1,0:T(8,128)(2,1)S(1)} %copy-done.1, bf16[2048,1024]{1,0:T(8,128)(2,1)} %param.25), kind=kOutput, calls=%fused_computation.17 | convolution fusion | flops 100687872 | bytes 4341760 | tf_op jit(solution)/shard_map/dot_general | solution.py:16
  14.1 8.6 %fusion.59 = f32[24,4,1,256]{3,2,1,0:T(1,128)S(1)} fusion(f32[24,4,128,1]{2,3,1,0:T(1,128)S(1)} %bitcast.82, f32[24,4,128,256]{3,2,1,0:T(8,128)} %param.22), kind=kOutput, calls=%fused_computation.89 | convolution fusion | flops 37748736 | bytes 12730368 | tf_op jit(solution)/shard_map/bhk,bhkv->bhv/dot_general | solution.py:64
  22.8 0.2 multiply_reduce_fusion
  23.0 2.8 %convolution_convert_fusion.2 = bf16[24,1024]{1,0:T(8,128)(2,1)S(1)} fusion(bf16[24,2048]{1,0:T(8,128)(2,1)S(1)} %copy-done.1, bf16[2048,1024]{1,0:T(8,128)(2,1)} %param.26), kind=kOutput, calls=%fused_computation.16 | convolution fusion | flops 100687872 | bytes 4341760 | tf_op jit(solution)/shard_map/dot_general | solution.py:16
  26.1 3.5 %convolution_convert_fusion = bf16[24,2048]{1,0:T(8,128)(2,1)} fusion(bf16[24,1024]{1,0:T(8,128)(2,1)S(1)} %bitcast.83, bf16[1024,2048]{1,0:T(8,128)(2,1)} %param.31), kind=kOutput, calls=%fused_computation | convolution fusion | flops 100712448 | bytes 4341760 | tf_op jit(solution)/shard_map/dot_general | solution.py:16
  29.9 0.6 reduce-window.6
  30.4 0.2 slice_reduce_fusion
  30.8 21.4 %reduce-scatter.2.cloned.1.call-done = bf16[24,512]{1,0:T(8,128)(2,1)} async-done(((bf16[24,2048]{1,0:T(8,128)(2,1)}), bf16[24,512]{1,0:T(8,128)(2,1)}) %reduce-scatter.2.cloned.1.call-update) | async-done | bytes 24592 | tf_op jit(solution)/shard_map/reduce_scatter | solution.py:76
  52.2 0.9 fusion.51
  53.0 5.8 %all-reduce.2 = (f32[24]{0:T(128)S(1)}, f32[24]{0:T(128)S(1)}) all-reduce(f32[24]{0:T(128)S(1)} %get-tuple-element.6, f32[24]{0:T(128)S(1)} %get-tuple-element.5), channel_id=1, replica_groups=mesh['ep'=8,'tp'=4] {'tp'}, use_global_device_ids=true, to_apply=%region_6.7 | all-reduce | flops 48 | bytes 384 | tf_op jit(solution)/shard_map/psum | solution.py:82
  58.8 0.8 multiply_convert_fusion.1
  59.7 0.3 convolution_convert_fusion.1
  60.1 0.7 copy.52
  60.9 5.7 %all-to-all-start = ((bf16[8,4,5,512]{3,1,2,0:T(4,128)(2,1)}), bf16[8,4,5,512]{3,1,2,0:T(4,128)(2,1)S(1)}, u32[]{:S(2)}, u32[]{:S(2)}) async-start(bf16[8,4,5,512]{3,1,2,0:T(4,128)(2,1)} %copy.52), calls=%async_computation.1 | async-start | bytes 327680 | tf_op jit(solution)/shard_map/all_to_all | solution.py:105
  66.8 7.3 %all-to-all-done = bf16[8,4,5,512]{3,1,2,0:T(4,128)(2,1)S(1)} async-done(((bf16[8,4,5,512]{3,1,2,0:T(4,128)(2,1)}), bf16[8,4,5,512]{3,1,2,0:T(4,128)(2,1)S(1)}, u32[]{:S(2)}, u32[]{:S(2)}) %all-to-all-start) | async-done | bytes 163872 | tf_op jit(solution)/shard_map/all_to_all | solution.py:105
  74.1 0.4 fusion.19
  74.5 7.2 %all-gather = bf16[32,4,5,512]{3,0,2,1:T(8,128)(2,1)S(1)} all-gather(bf16[8,4,5,512]{3,0,2,1:T(8,128)(2,1)S(1)} %fusion.19), channel_id=2, replica_groups=mesh['ep'=8,'tp'=4] {'tp'}, dimensions={0}, use_global_device_ids=true | all-gather | bytes 819200 | tf_op jit(solution)/shard_map/all_gather | solution.py:112
  81.7 1.1 fusion.22
  82.9 29.9 %all-reduce.6.cloned.1.call-done = bf16[8,4,5,512]{3,0,2,1:T(8,128)(2,1)} async-done(((bf16[8,4,5,512]{3,0,2,1:T(8,128)(2,1)}), bf16[8,4,5,512]{3,0,2,1:T(8,128)(2,1)}) %all-reduce.6.cloned.1.call-update) | async-done | bytes 163856 | tf_op jit(solution)/shard_map/psum | solution.py:111
  112.8 2.1 %fusion.16 = bf16[8,4,5,512]{3,0,2,1:T(8,128)(2,1)S(1)} fusion(bf16[4,512,512]{2,1,0:T(8,128)(2,1)} %param.37, bf16[8,4,5,512]{3,0,2,1:T(8,128)(2,1)S(1)} %bitcast_reduce_fusion, bf16[8,4,5,512]{3,0,2,1:T(8,128)(2,1)} %all-reduce.6.cloned.1.call-done), kind=kOutput, calls=%fused_computation.13 | convolution fusion | flops 84623360 | bytes 2588672 | tf_op jit(solution)/shard_map/secf,efd->secd/dot_general | solution.py:120
  114.9 0.7 copy.55
  115.6 5.5 %all-to-all-start.1 = ((bf16[8,4,5,512]{3,1,2,0:T(4,128)(2,1)}), bf16[8,4,5,512]{3,1,2,0:T(4,128)(2,1)S(1)}, u32[]{:S(2)}, u32[]{:S(2)}) async-start(bf16[8,4,5,512]{3,1,2,0:T(4,128)(2,1)} %copy.55), calls=%async_computation.2 | async-start | bytes 327680 | tf_op jit(solution)/shard_map/all_to_all | solution.py:123
  121.2 1.2 convolution_convert_fusion.6
  122.4 1.2 convolution_convert_fusion.7
  123.6 10.9 %all-reduce.3 = (bf16[24,512]{1,0:T(8,128)(2,1)S(1)}, bf16[24,512]{1,0:T(8,128)(2,1)S(1)}) all-reduce(bf16[24,512]{1,0:T(8,128)(2,1)S(1)} %convolution_convert_fusion.6, bf16[24,512]{1,0:T(8,128)(2,1)S(1)} %convolution_convert_fusion.7), channel_id=1, replica_groups=mesh['ep'=8,'tp'=4] {'tp'}, use_global_device_ids=true, to_apply=%region_14.15 | all-reduce | flops 24576 | bytes 98304 | tf_op jit(solution)/shard_map/psum | solution.py:114
  134.6 0.2 fusion.15
  134.9 1.3 fusion.58
  136.2 5.9 %all-reduce.1 = (f32[24]{0:T(128)S(1)}, f32[24]{0:T(128)S(1)}) all-reduce(f32[24]{0:T(128)S(1)} %get-tuple-element.8, f32[24]{0:T(128)S(1)} %get-tuple-element.7), channel_id=1, replica_groups=mesh['ep'=8,'tp'=4] {'tp'}, use_global_device_ids=true, to_apply=%region_18.19 | all-reduce | flops 48 | bytes 384 | tf_op jit(solution)/shard_map/psum | solution.py:133
  142.1 0.7 multiply_convert_fusion
  (57 shorter events, 1.7 us)
Async XLA Ops:
  6.5 67.6 %copy-start = (bf16[4,512,512]{2,1,0:T(8,128)(2,1)S(1)}, bf16[4,512,512]{2,1,0:T(8,128)(2,1)}, u32[]{:S(2)}) copy-start(bf16[4,512,512]{2,1,0:T(8,128)(2,1)} %param.36) | copy-start | bytes 6291460
  6.5 2.2 %copy-start.1 = (bf16[24,2048]{1,0:T(8,128)(2,1)S(1)}, bf16[24,2048]{1,0:T(8,128)(2,1)}, u32[]{:S(2)}) copy-start(bf16[24,2048]{1,0:T(8,128)(2,1)} %param.21) | copy-start | bytes 294916
  6.5 2.2 %copy-start.3 = (bf16[2048,16]{0,1:T(8,128)(2,1)S(1)}, bf16[2048,16]{0,1:T(8,128)(2,1)}, u32[]{:S(2)}) copy-start(bf16[2048,16]{0,1:T(8,128)(2,1)} %param.27) | copy-start | bytes 196612
  6.5 2.4 %copy-start.8 = (bf16[16,512]{1,0:T(8,128)(2,1)S(1)}, bf16[16,512]{1,0:T(8,128)(2,1)}, u32[]{:S(2)}) copy-start(bf16[16,512]{1,0:T(8,128)(2,1)} %param.28) | copy-start | bytes 49156
  6.5 2.4 %copy-start.10 = (f32[512]{0:T(512)S(1)}, f32[512]{0:T(512)}, u32[]{:S(2)}) copy-start(f32[512]{0:T(512)} %param.29) | copy-start | bytes 6148
  6.5 45.6 %reduce-scatter.2.cloned.1.call-start = ((), (), s32[]{:S(2)}) async-start(), calls=%async_computation.3 | async-start | bytes 122880 | tf_op jit(solution)/shard_map/reduce_scatter | solution.py:76
  23.0 2.9 %copy-start.7 = (f32[256]{0:T(256)S(1)}, f32[256]{0:T(256)}, u32[]{:S(2)}) copy-start(f32[256]{0:T(256)} %param.30) | copy-start | bytes 3076
  26.1 3.5 %copy-start.4 = (s32[24,6]{0,1:T(8,128)S(1)}, s32[24,6]{0,1:T(8,128)}, u32[]{:S(2)}) copy-start(s32[24,6]{0,1:T(8,128)} %param.33) | copy-start | bytes 1732
  26.1 32.7 %copy-start.5 = (f32[512]{0:T(512)S(1)}, f32[512]{0:T(512)}, u32[]{:S(2)}) copy-start(f32[512]{0:T(512)} %param.32) | copy-start | bytes 6148
  60.9 13.2 %all-to-all-start = ((bf16[8,4,5,512]{3,1,2,0:T(4,128)(2,1)}), bf16[8,4,5,512]{3,1,2,0:T(4,128)(2,1)S(1)}, u32[]{:S(2)}, u32[]{:S(2)}) async-start(bf16[8,4,5,512]{3,1,2,0:T(4,128)(2,1)} %copy.52), calls=%async_computation.1 | async-start | bytes 327680 | tf_op jit(solution)/shard_map/all_to_all | solution.py:105
  66.5 46.2 %all-reduce.6.cloned.1.call-start = ((), (), s32[]{:S(2)}) async-start(), calls=%async_computation.4 | async-start | bytes 327680 | tf_op jit(solution)/shard_map/psum | solution.py:111
  74.1 7.6 %copy-start.2 = (bf16[4,512,512]{2,1,0:T(8,128)(2,1)S(1)}, bf16[4,512,512]{2,1,0:T(8,128)(2,1)}, u32[]{:S(2)}) copy-start(bf16[4,512,512]{2,1,0:T(8,128)(2,1)} %param.35) | copy-start | bytes 6291460
  82.9 51.7 %copy-start.9 = (f32[24,6]{0,1:T(8,128)S(1)}, f32[24,6]{0,1:T(8,128)}, u32[]{:S(2)}) copy-start(f32[24,6]{0,1:T(8,128)} %param.34) | copy-start | bytes 1732
  114.9 27.2 %copy-start.6 = (f32[512]{0:T(512)S(1)}, f32[512]{0:T(512)}, u32[]{:S(2)}) copy-start(f32[512]{0:T(512)} %param.41) | copy-start | bytes 6148
  115.6 18.8 %all-to-all-start.1 = ((bf16[8,4,5,512]{3,1,2,0:T(4,128)(2,1)}), bf16[8,4,5,512]{3,1,2,0:T(4,128)(2,1)S(1)}, u32[]{:S(2)}, u32[]{:S(2)}) async-start(bf16[8,4,5,512]{3,1,2,0:T(4,128)(2,1)} %copy.55), calls=%async_computation.2 | async-start | bytes 327680 | tf_op jit(solution)/shard_map/all_to_all | solution.py:123
Sparse Core Ops, SparseCore 0:
  29.7 22.3 reduce-scatter.1
  82.9 29.8 all-reduce.5
